TPU v7x, 512 devices: a whole 4x8x8 slice. The times are simulated.
512 devices in a mesh: rep: 2 (over z_hi), fs: 32 (over z_lo, y), tp: 8 (over x, core).
Axes of the slice: x: 4, y: 8, z: 8 (z_hi: 2, z_lo: 4; z = z_hi * 4 + z_lo), core: 2. Of those that a mesh axis runs over, the one named last changes fastest.
Arguments:
- x_later: bfloat16 [8192, 2048], P(('rep', 'fs')), may hold values from -6 to 6
- kept_input_rows: bfloat16 [8192, 2048], P(('rep', 'fs')), may hold values from -6 to 6
- cotangent: bfloat16 [8192, 2048], P(('rep', 'fs')), may hold values from -8 to 8
- norm_gain_vector: float32 [2048], replicated, may hold values from 0.1 to 1.9
- up_weight: bfloat16 [2048, 4096], P('fs', 'tp'), may hold values from -0.125 to 0.125
- down_weight: bfloat16 [4096, 2048], P('tp', 'fs'), may hold values from -0.09375 to 0.09375
- up_sum: float32 [2048, 4096], P('fs', 'tp'), may hold values from -6 to 6
- down_sum: float32 [4096, 2048], P('tp', 'fs'), may hold values from -6 to 6
Outputs:
- mixed: bfloat16 [8192, 2048], P(('rep', 'fs'))
- input_gradient_rows: bfloat16 [8192, 2048], P(('rep', 'fs'))
- up_total: float32 [2048, 4096], P('fs', 'tp')
- down_total: float32 [4096, 2048], P('tp', 'fs')
All inputs are finite; a program needn't handle non-finite values.
Results may differ from a plain program's by a relative error of at most 0.018.
Values may be sent and summed in bfloat16 or wider, within the bound.
No kernel may reach another device: no remote copies, remote signals or barrier semaphores. Data moves between devices by JAX's collectives and lax.ppermute only.
A program may use at most 64 MiB of HBM per device.

v0:
```python
import jax
import jax.numpy as jnp
from jax import lax
from jax.sharding import Mesh
from jax.sharding import PartitionSpec as P

FS = ("fs_0", "fs_1")
REP_FS = ("rep", "fs_0", "fs_1")
EPSILON = 1e-06
TRANSPOSED = (((1,), (1,)), ((), ()))
LEADING = (((0,), (0,)), ((), ()))


def sent_to_all(shard, axis):
    copies = jnp.broadcast_to(shard, (lax.axis_size(axis), *shard.shape))
    return lax.all_to_all(copies, axis, split_axis=0, concat_axis=0, tiled=True)


def in_order(tiles, dim):
    lengths = list(tiles.shape[1:])
    lengths[dim] *= tiles.shape[0]
    return jnp.moveaxis(tiles, 0, dim).reshape(lengths)


def gathered_copies(shard, axis, dim):
    tiles = sent_to_all(shard, axis)
    return in_order(tiles, dim)


def together(arrays, axis):
    ends = [0]
    for a in arrays:
        ends.append(ends[-1] + a.size)
    subtotal = lax.psum(jnp.concatenate([a.ravel() for a in arrays]), axis)
    return tuple((subtotal[b:e].reshape(a.shape) for a, b, e in zip(arrays, ends, ends[1:])))


def all_blocks(shard, axes, order):
    tiles = shard[None]
    for k in order:
        tiles = lax.all_gather(tiles, axes[k], axis=0, tiled=True)
    held = [lax.axis_size(axes[k]) for k in reversed(order)]
    tiles = tiles.reshape(*held, *shard.shape)
    turned = sorted(range(len(order)), key=lambda place: order[len(order) - 1 - place])
    return tiles.transpose(*turned, *range(len(order), tiles.ndim)).reshape(-1, *shard.shape)


def gathered_by_axis(shard, axes, order, dim):
    return in_order(all_blocks(shard, axes, order), dim)


def over_copies(shard, axis):
    return sent_to_all(shard, axis).astype(jnp.float32).sum(axis=0)


def norm_partial_terms(values, norm_gain_vector):
    floats = values.astype(jnp.float32)
    inverse = lax.rsqrt(jnp.mean(floats * floats, axis=-1, keepdims=True) + EPSILON)
    unit_rows = floats * inverse
    normed = (unit_rows * norm_gain_vector).astype(jnp.bfloat16)
    return (inverse, unit_rows, normed)


def squared_relu(pre_act):
    return jnp.square(jax.nn.relu(pre_act)).astype(jnp.bfloat16)


def body(
    x_later, kept_input_rows, cotangent, norm_gain_vector, up_weight, down_weight, up_sum, down_sum
):
    row_count = x_later.shape[0]
    grad_scale = float(row_count * lax.axis_size("rep") * lax.axis_size(FS)) ** (-0.5)
    inv_later, unit_later, normed_later = norm_partial_terms(x_later, norm_gain_vector)
    inverse_rms_kept, unit_kept_rows, normed_kept_rows = norm_partial_terms(
        kept_input_rows, norm_gain_vector
    )
    stacked = jnp.concatenate([normed_kept_rows, normed_later], axis=0)
    columns = stacked
    pre_act = jnp.dot(
        columns, gathered_copies(up_weight, FS, 0), preferred_element_type=jnp.float32
    )
    pre_saved = pre_act[:row_count]
    hidden_saved = squared_relu(pre_saved)
    hidden_later = squared_relu(pre_act[row_count:])
    shard_part = gathered_copies(down_weight, FS, 1)
    product = jnp.dot(hidden_later, shard_part, preferred_element_type=jnp.float32)
    columns = cotangent
    grad_acc = lax.dot_general(columns, shard_part, TRANSPOSED, preferred_element_type=jnp.float32)
    pre_grad = (grad_acc * 2.0 * jax.nn.relu(pre_saved)).astype(jnp.bfloat16)
    back_part = lax.dot_general(
        pre_grad, gathered_copies(up_weight, FS, 0), TRANSPOSED, preferred_element_type=jnp.float32
    )
    mixed_sum, back_sum = tuple(
        (
            part.astype(jnp.float32)
            for part in together(
                (product.astype(jnp.bfloat16), back_part.astype(jnp.bfloat16)), "tp"
            )
        )
    )
    mixed = mixed_sum.astype(jnp.bfloat16)
    scaled_rows = back_sum * norm_gain_vector
    input_gradient_rows = (
        inverse_rms_kept
        * (
            scaled_rows
            - unit_kept_rows * jnp.mean(scaled_rows * unit_kept_rows, axis=-1, keepdims=True)
        )
    ).astype(jnp.bfloat16)
    cot_columns, normed_columns = (
        lax.all_to_all(cotangent, FS, split_axis=1, concat_axis=0, tiled=True),
        lax.all_to_all(normed_kept_rows, FS, split_axis=1, concat_axis=0, tiled=True),
    )
    columns = normed_columns
    up_grad = grad_scale * lax.dot_general(
        columns,
        gathered_by_axis(pre_grad, FS, (0, 1), 0),
        LEADING,
        preferred_element_type=jnp.float32,
    )
    columns = cot_columns
    down_grad = lax.dot_general(
        gathered_by_axis(hidden_saved, FS, (0, 1), 0),
        columns,
        LEADING,
        preferred_element_type=jnp.float32,
    )
    up_added, down_added = (
        over_copies(up_grad.astype(jnp.bfloat16), "rep").astype(jnp.float32),
        over_copies((down_grad * grad_scale).astype(jnp.bfloat16), "rep").astype(jnp.float32),
    )
    return (mixed, input_gradient_rows, up_sum + up_added, down_sum + down_added)


def solution(mesh):
    finer = Mesh(
        mesh.devices.reshape(mesh.shape["rep"], 4, 8, mesh.shape["tp"]),
        ("rep", "fs_0", "fs_1", "tp"),
    )
    return jax.shard_map(
        body,
        mesh=finer,
        in_specs=(
            P(REP_FS, None),
            P(REP_FS, None),
            P(REP_FS, None),
            P(),
            P(FS, "tp"),
            P("tp", FS),
            P(FS, "tp"),
            P("tp", FS),
        ),
        out_specs=(P(REP_FS, None), P(REP_FS, None), P(FS, "tp"), P("tp", FS)),
        check_vma=False,
    )
```

profile of v0, /device:TPU:2, one launch (start us, length us, event | category | flops | bytes accessed | tf_op | source)
XLA Modules:
  0.0 325.3 jit_solution(14748956280166571231)
XLA Ops:
  8.0 1.1 broadcast_in_dim.12
  9.1 64.7 %all_to_all.59 = bf16[32,64,512]{2,1,0:T(8,128)(2,1)} all-to-all(bf16[32,64,512]{2,1,0:T(8,128)(2,1)S(1)} %broadcast_in_dim.12), channel_id=1, replica_groups=mesh['rep'=2,'fs_0'=4,'fs_1'=8,'tp'=8] {'fs_0','fs_1'}, dimensions={0} | all-to-all | bytes 4194304 | tf_op jit(solution)/shard_map/all_to_all | solution.py:16
  73.8 1.5 broadcast_in_dim.26
  75.3 4.5 %all-to-all-start.1 = ((bf16[32,512,64]{1,2,0:T(8,128)(2,1)}), bf16[32,512,64]{1,2,0:T(8,128)(2,1)S(1)}, u32[]{:S(2)}, u32[]{:S(2)}) async-start(bf16[32,512,64]{1,2,0:T(8,128)(2,1)} %broadcast_in_dim.26), calls=%async_computation.1 | async-start | bytes 4194304 | tf_op jit(solution)/shard_map/all_to_all | solution.py:16
  80.6 0.8 copy-done.8
  81.5 1.5 fusion.18
  83.0 51.5 %all-to-all-done.1 = bf16[32,512,64]{1,2,0:T(8,128)(2,1)S(1)} async-done(((bf16[32,512,64]{1,2,0:T(8,128)(2,1)}), bf16[32,512,64]{1,2,0:T(8,128)(2,1)S(1)}, u32[]{:S(2)}, u32[]{:S(2)}) %all-to-all-start.1) | async-done | bytes 2097184 | tf_op jit(solution)/shard_map/all_to_all | solution.py:16
  134.5 1.8 fusion.3
  136.8 1.1 copy-done.2
  137.9 0.8 fusion.4
  139.0 1.1 pad_maximum_fusion
  140.2 15.7 %all-gather = bf16[512,512]{1,0:T(8,128)(2,1)} all-gather(bf16[128,512]{1,0:T(8,128)(2,1)S(1)} %fusion.6), channel_id=2, replica_groups=mesh['rep'=2,'fs_0'=4,'fs_1'=8,'tp'=8] {'fs_0'}, dimensions={0}, use_global_device_ids=true | all-gather | bytes 655360 | tf_op jit(solution)/shard_map/all_gather | solution.py:41
  155.9 1.0 copy.34
  156.9 5.6 %all-to-all-start.2 = ((bf16[128,32,64]{0,2,1:T(8,128)(2,1)}), bf16[128,32,64]{0,2,1:T(8,128)(2,1)S(1)}, u32[]{:S(2)}, u32[]{:S(2)}) async-start(bf16[128,32,64]{0,2,1:T(8,128)(2,1)} %bitcast.4), calls=%async_computation.2 | async-start | bytes 1048576 | tf_op jit(solution)/shard_map/all_to_all | solution.py:112
  162.5 1.0 copy.38
  163.6 21.1 %all-gather.1 = bf16[512,512]{1,0:T(8,128)(2,1)} all-gather(bf16[128,512]{1,0:T(8,128)(2,1)S(1)} %multiply_convert_fusion), channel_id=3, replica_groups=mesh['rep'=2,'fs_0'=4,'fs_1'=8,'tp'=8] {'fs_0'}, dimensions={0}, use_global_device_ids=true | all-gather | bytes 655360 | tf_op jit(solution)/shard_map/all_gather | solution.py:41
  184.8 8.8 %all-to-all-start.4 = ((bf16[128,32,64]{0,2,1:T(8,128)(2,1)}), bf16[128,32,64]{0,2,1:T(8,128)(2,1)}, u32[]{:S(2)}, u32[]{:S(2)}) async-start(bf16[128,32,64]{0,2,1:T(8,128)(2,1)} %bitcast.14), calls=%async_computation.4 | async-start | bytes 1048576 | tf_op jit(solution)/shard_map/all_to_all | solution.py:111
  193.5 16.0 %all-reduce.2.cloned.1.call-done = bf16[524288]{0:T(1024)(128)(2,1)} async-done(((bf16[524288]{0:T(1024)(128)(2,1)}), bf16[524288]{0:T(1024)(128)(2,1)}) %all-reduce.2.cloned.1.call-update) | async-done | bytes 1048592 | tf_op jit(solution)/shard_map/psum | solution.py:34
  209.6 2.1 slice_convert_fusion
  212.1 12.9 %all-gather.5.cloned.1.call-done = bf16[32,128,512]{2,1,0:T(8,128)(2,1)} async-done(((bf16[4,128,512]{2,1,0:T(8,128)(2,1)}), bf16[32,128,512]{2,1,0:T(8,128)(2,1)}) %all-gather.5.cloned.1.call-update) | async-done | bytes 4194320 | tf_op jit(solution)/shard_map/all_gather | solution.py:41
  225.0 4.6 %copy.36 = bf16[4,8,128,512]{3,2,1,0:T(8,128)(2,1)} copy(bf16[4,8,128,512]{3,2,0,1:T(8,128)(2,1)} %bitcast.52) | data formatting | bytes 8388608 | tf_op jit(solution)/shard_map/transpose | solution.py:45
  229.6 53.1 %all-gather.7.cloned.1.call-done = bf16[32,128,512]{2,1,0:T(8,128)(2,1)} async-done(((bf16[4,128,512]{2,1,0:T(8,128)(2,1)}), bf16[32,128,512]{2,1,0:T(8,128)(2,1)}) %all-gather.7.cloned.1.call-update) | async-done | bytes 4194320 | tf_op jit(solution)/shard_map/all_gather | solution.py:41
  282.8 4.7 %copy.37 = bf16[4,8,128,512]{3,2,1,0:T(8,128)(2,1)} copy(bf16[4,8,128,512]{3,2,0,1:T(8,128)(2,1)} %bitcast.53) | data formatting | bytes 8388608 | tf_op jit(solution)/shard_map/transpose | solution.py:45
  287.5 0.8 fusion.7
  289.0 7.4 %all-to-all-start.3 = ((bf16[2,64,512]{2,1,0:T(8,128)(2,1)}), bf16[2,64,512]{2,1,0:T(8,128)(2,1)S(1)}, u32[]{:S(2)}, u32[]{:S(2)}) async-start(bf16[2,64,512]{2,1,0:T(8,128)(2,1)} %broadcast_in_dim.28), calls=%async_computation.3 | async-start | bytes 262144 | tf_op jit(solution)/shard_map/all_to_all | solution.py:16
  296.4 3.2 fusion.8
  299.6 5.2 %all-to-all-done.3 = bf16[2,64,512]{2,1,0:T(8,128)(2,1)S(1)} async-done(((bf16[2,64,512]{2,1,0:T(8,128)(2,1)}), bf16[2,64,512]{2,1,0:T(8,128)(2,1)S(1)}, u32[]{:S(2)}, u32[]{:S(2)}) %all-to-all-start.3) | async-done | bytes 131104 | tf_op jit(solution)/shard_map/all_to_all | solution.py:16
  305.4 3.4 %all-to-all-start.5 = ((bf16[2,512,64]{1,2,0:T(8,128)(2,1)}), bf16[2,512,64]{1,2,0:T(8,128)(2,1)S(1)}, u32[]{:S(2)}, u32[]{:S(2)}) async-start(bf16[2,512,64]{1,2,0:T(8,128)(2,1)} %broadcast_in_dim.30), calls=%async_computation.5 | async-start | bytes 262144 | tf_op jit(solution)/shard_map/all_to_all | solution.py:16
  308.8 1.1 fusion.13
  310.0 1.0 slice.33
  311.0 0.7 add.26
  311.7 5.5 %all-to-all-done.5 = bf16[2,512,64]{1,2,0:T(8,128)(2,1)S(1)} async-done(((bf16[2,512,64]{1,2,0:T(8,128)(2,1)}), bf16[2,512,64]{1,2,0:T(8,128)(2,1)S(1)}, u32[]{:S(2)}, u32[]{:S(2)}) %all-to-all-start.5) | async-done | bytes 131104 | tf_op jit(solution)/shard_map/all_to_all | solution.py:16
  (54 shorter events, 4.2 us)
Async XLA Ops:
  9.1 64.7 %copy-start.15 = (bf16[512,64]{0,1:T(8,128)(2,1)S(1)}, bf16[512,64]{0,1:T(8,128)(2,1)}, u32[]{:S(2)}) copy-start(bf16[512,64]{0,1:T(8,128)(2,1)} %param.13) | copy-start | bytes 196612
  75.3 4.6 %copy-start.3 = (bf16[128,2048]{1,0:T(8,128)(2,1)S(1)}, bf16[128,2048]{1,0:T(8,128)(2,1)}, u32[]{:S(2)}) copy-start(bf16[128,2048]{1,0:T(8,128)(2,1)} %param.9) | copy-start | bytes 1572868
  75.3 4.8 %copy-start.5 = (bf16[128,2048]{1,0:T(8,128)(2,1)S(1)}, bf16[128,2048]{1,0:T(8,128)(2,1)}, u32[]{:S(2)}) copy-start(bf16[128,2048]{1,0:T(8,128)(2,1)} %param.8) | copy-start | bytes 1572868
  75.3 5.0 %copy-start.14 = (f32[2048]{0:T(1024)S(1)}, f32[2048]{0:T(1024)}, u32[]{:S(2)}) copy-start(f32[2048]{0:T(1024)} %param.11) | copy-start | bytes 24580
  75.3 59.2 %all-to-all-start.1 = ((bf16[32,512,64]{1,2,0:T(8,128)(2,1)}), bf16[32,512,64]{1,2,0:T(8,128)(2,1)S(1)}, u32[]{:S(2)}, u32[]{:S(2)}) async-start(bf16[32,512,64]{1,2,0:T(8,128)(2,1)} %broadcast_in_dim.26), calls=%async_computation.1 | async-start | bytes 4194304 | tf_op jit(solution)/shard_map/all_to_all | solution.py:16
  79.8 129.7 %all-reduce.2.cloned.1.call-start = ((), (), s32[]{:S(2)}) async-start(), calls=%async_computation.6 | async-start | bytes 2097152 | tf_op jit(solution)/shard_map/psum | solution.py:34
  79.9 1.6 copy-start.1
  80.6 0.8 copy-start.8
  83.0 53.4 %copy-start.6 = (bf16[128,2048]{1,0:T(8,128)(2,1)S(1)}, bf16[128,2048]{1,0:T(8,128)(2,1)}, u32[]{:S(2)}) copy-start(bf16[128,2048]{1,0:T(8,128)(2,1)} %param.10) | copy-start | bytes 1572868
  134.5 1.9 copy-start.10
  136.3 1.6 copy-start.2
  139.0 16.9 %copy-start.9 = (bf16[128,2048]{1,0:T(8,128)(2,1)S(1)}, bf16[128,2048]{1,0:T(8,128)(2,1)}, u32[]{:S(2)}) copy-start(bf16[128,2048]{1,0:T(8,128)(2,1)} %copy-done.8) | copy-start | bytes 1572868
  140.1 22.5 %copy-start.7 = (bf16[128,2048]{1,0:T(8,128)(2,1)S(1)}, bf16[128,2048]{1,0:T(8,128)(2,1)}, u32[]{:S(2)}) copy-start(bf16[128,2048]{1,0:T(8,128)(2,1)} %param.10) | copy-start | bytes 1572868
  140.1 23.5 %copy-start.11 = (f32[256,512]{1,0:T(8,128)S(1)}, f32[256,512]{1,0:T(8,128)}, u32[]{:S(2)}) copy-start(f32[256,512]{1,0:T(8,128)} %fusion.18) | copy-start | bytes 1572868
  140.1 84.9 %all-gather.5.cloned.1.call-start = ((), (), s32[]{:S(2)}) async-start(), calls=%async_computation.7 | async-start | bytes 4718592 | tf_op jit(solution)/shard_map/all_gather | solution.py:41
  156.9 27.9 %all-to-all-start.2 = ((bf16[128,32,64]{0,2,1:T(8,128)(2,1)}), bf16[128,32,64]{0,2,1:T(8,128)(2,1)S(1)}, u32[]{:S(2)}, u32[]{:S(2)}) async-start(bf16[128,32,64]{0,2,1:T(8,128)(2,1)} %bitcast.4), calls=%async_computation.2 | async-start | bytes 1048576 | tf_op jit(solution)/shard_map/all_to_all | solution.py:112
  162.5 120.3 %all-gather.7.cloned.1.call-start = ((), (), s32[]{:S(2)}) async-start(), calls=%async_computation.8 | async-start | bytes 4718592 | tf_op jit(solution)/shard_map/all_gather | solution.py:41
  184.8 103.6 %all-to-all-start.4 = ((bf16[128,32,64]{0,2,1:T(8,128)(2,1)}), bf16[128,32,64]{0,2,1:T(8,128)(2,1)}, u32[]{:S(2)}, u32[]{:S(2)}) async-start(bf16[128,32,64]{0,2,1:T(8,128)(2,1)} %bitcast.14), calls=%async_computation.4 | async-start | bytes 1048576 | tf_op jit(solution)/shard_map/all_to_all | solution.py:111
  282.8 4.7 %copy-start = (bf16[4,8,128,512]{3,2,1,0:T(8,128)(2,1)S(1)}, bf16[4,8,128,512]{3,2,1,0:T(8,128)(2,1)}, u32[]{:S(2)}) copy-start(bf16[4,8,128,512]{3,2,1,0:T(8,128)(2,1)} %copy.36) | copy-start | bytes 12582916
  289.0 15.7 %all-to-all-start.3 = ((bf16[2,64,512]{2,1,0:T(8,128)(2,1)}), bf16[2,64,512]{2,1,0:T(8,128)(2,1)S(1)}, u32[]{:S(2)}, u32[]{:S(2)}) async-start(bf16[2,64,512]{2,1,0:T(8,128)(2,1)} %broadcast_in_dim.28), calls=%async_computation.3 | async-start | bytes 262144 | tf_op jit(solution)/shard_map/all_to_all | solution.py:16
  299.6 10.4 %copy-start.4 = (bf16[262144]{0:T(1024)(128)(2,1)S(1)}, bf16[262144]{0:T(1024)(128)(2,1)}, u32[]{:S(2)}) copy-start(bf16[262144]{0:T(1024)(128)(2,1)} %get-tuple-element.9) | copy-start | bytes 1572868
  299.6 11.4 %copy-start.12 = (f32[64,512]{1,0:T(8,128)S(1)}, f32[64,512]{1,0:T(8,128)}, u32[]{:S(2)}) copy-start(f32[64,512]{1,0:T(8,128)} %param.14) | copy-start | bytes 393220
  305.4 11.8 %all-to-all-start.5 = ((bf16[2,512,64]{1,2,0:T(8,128)(2,1)}), bf16[2,512,64]{1,2,0:T(8,128)(2,1)S(1)}, u32[]{:S(2)}, u32[]{:S(2)}) async-start(bf16[2,512,64]{1,2,0:T(8,128)(2,1)} %broadcast_in_dim.30), calls=%async_computation.5 | async-start | bytes 262144 | tf_op jit(solution)/shard_map/all_to_all | solution.py:16
  308.8 8.4 %copy-start.13 = (f32[512,64]{0,1:T(8,128)S(1)}, f32[512,64]{0,1:T(8,128)}, u32[]{:S(2)}) copy-start(f32[512,64]{0,1:T(8,128)} %param.15) | copy-start | bytes 393220
Sparse Core Ops, SparseCore 0:
  140.2 69.2 all-reduce.1
Sparse Core Ops, SparseCore 1:
  156.0 69.0 all-gather.4
  227.0 55.7 all-gather.6
where the time goes:
time: 326 us; the launch traced here: 325 us
  waiting for transfers between devices  144 us (44%)
  blocking collectives  101 us (31%)
  starting transfers between devices  29.7 us (9%)
  local copies, waits for them, and re-layouts  18.8 us (6%)
  between operations  15.8 us (5%)
  matrix products  8.61 us (3%)
  other arithmetic  6.7 us (2%)
    all_gather x2, waiting for transfers between devices, all_blocks(): tiles = lax.all_gather(tiles, axes[k], axis=0, tiled=True)  66 us
    all_to_all x1, blocking collectives, sent_to_all(): return lax.all_to_all(copies, axis, split_axis=0, concat_axis=0, tiled=True)  64.7 us
    all_to_all x3, waiting for transfers between devices, sent_to_all(): return lax.all_to_all(copies, axis, split_axis=0, concat_axis=0, tiled=True)  62.2 us
    all_gather x2, blocking collectives, all_blocks(): tiles = lax.all_gather(tiles, axes[k], axis=0, tiled=True)  36.8 us
    psum x1, waiting for transfers between devices, together(): subtotal = lax.psum(jnp.concatenate([a.ravel() for a in arrays]), axis)  16 us
    all_to_all x3, starting transfers between devices, sent_to_all(): return lax.all_to_all(copies, axis, split_axis=0, concat_axis=0, tiled=True)  15.2 us
    transpose x2, local copies, waits for them, and re-layouts, all_blocks(): tiles.transpose(*turned, *range(len(order), tiles.ndim))  9.32 us
    all_to_all x1, starting transfers between devices, body(): lax.all_to_all(cotangent, FS, split_axis=1, concat_axis=0, tiled=True)  8.76 us
  transfers between devices with their start and end apart: 8, of which 6 were waited for; matrix products, arithmetic and copies ran while one was open for 7% of the time, Pallas kernels for 0%

commit v1 on v0

--- a/solution.py
+++ b/solution.py
@@ -9,6 +9,11 @@
 EPSILON = 1e-06
 TRANSPOSED = (((1,), (1,)), ((), ()))
 LEADING = (((0,), (0,)), ((), ()))
+
+
+def swapped_in(x, mesh_axis, dim):
+    sent = jnp.stack([x] * lax.axis_size(mesh_axis))
+    return jnp.concatenate(lax.all_to_all(sent, mesh_axis, 0, 0), axis=dim)
 
 
 def sent_to_all(shard, axis):
@@ -38,7 +43,7 @@
 def all_blocks(shard, axes, order):
     tiles = shard[None]
     for k in order:
-        tiles = lax.all_gather(tiles, axes[k], axis=0, tiled=True)
+        tiles = swapped_in(tiles, axes[k], 0)
     held = [lax.axis_size(axes[k]) for k in reversed(order)]
     tiles = tiles.reshape(*held, *shard.shape)
     turned = sorted(range(len(order)), key=lambda place: order[len(order) - 1 - place])

time: 326 us -> 458 us (1.40)
  the two profiles are of different devices: /device:TPU:2 before, /device:TPU:14 now
where the time goes in v1:
time: 458 us; the launch traced here: 456 us
  waiting for transfers between devices  272 us (59%)
  blocking collectives  79.9 us (17%)
  starting transfers between devices  46 us (10%)
  local copies, waits for them, and re-layouts  25.3 us (6%)
  between operations  14.3 us (3%)
  matrix products  10.4 us (2%)
  other arithmetic  8.58 us (2%)
    all_to_all x3, waiting for transfers between devices, swapped_in(): return jnp.concatenate(lax.all_to_all(sent, mesh_axis, 0, 0), axis=dim)  194 us
    all_to_all x1, blocking collectives, sent_to_all(): return lax.all_to_all(copies, axis, split_axis=0, concat_axis=0, tiled=True)  64.2 us
    all_to_all x3, waiting for transfers between devices, sent_to_all(): return lax.all_to_all(copies, axis, split_axis=0, concat_axis=0, tiled=True)  58.6 us
    all_to_all x3, starting transfers between devices, swapped_in(): return jnp.concatenate(lax.all_to_all(sent, mesh_axis, 0, 0), axis=dim)  16.7 us
    all_to_all x3, starting transfers between devices, sent_to_all(): return lax.all_to_all(copies, axis, split_axis=0, concat_axis=0, tiled=True)  16.1 us
    all_to_all x1, blocking collectives, swapped_in(): return jnp.concatenate(lax.all_to_all(sent, mesh_axis, 0, 0), axis=dim)  15.6 us
    all_to_all x1, waiting for transfers between devices, body(): lax.all_to_all(normed_kept_rows, FS, split_axis=1, concat_axis=0, tiled=T...  13.3 us
  transfers between devices with their start and end apart: 9, of which 8 were waited for; matrix products, arithmetic and copies ran while one was open for 7% of the time, Pallas kernels for 0%

profile of v1, /device:TPU:14, one launch (start us, length us, event | category | flops | bytes accessed | tf_op | source)
XLA Modules:
  0.0 456.5 jit_solution(7557668740248413795)
XLA Ops:
  7.2 1.1 broadcast_in_dim.8
  8.3 64.2 %all_to_all.79 = bf16[32,64,512]{2,1,0:T(8,128)(2,1)} all-to-all(bf16[32,64,512]{2,1,0:T(8,128)(2,1)S(1)} %broadcast_in_dim.8), channel_id=1, replica_groups=mesh['rep'=2,'fs_0'=4,'fs_1'=8,'tp'=8] {'fs_0','fs_1'}, dimensions={0} | all-to-all | bytes 4194304 | tf_op jit(solution)/shard_map/all_to_all | solution.py:21
  72.5 1.6 broadcast_in_dim.9
  74.1 5.1 %all-to-all-start.1 = ((bf16[32,512,64]{1,2,0:T(8,128)(2,1)}), bf16[32,512,64]{1,2,0:T(8,128)(2,1)S(1)}, u32[]{:S(2)}, u32[]{:S(2)}) async-start(bf16[32,512,64]{1,2,0:T(8,128)(2,1)} %broadcast_in_dim.9), calls=%async_computation.1 | async-start | bytes 4194304 | tf_op jit(solution)/shard_map/all_to_all | solution.py:21
  79.6 1.3 fusion.9
  80.9 2.1 copy.32
  82.9 47.9 %all-to-all-done.1 = bf16[32,512,64]{1,2,0:T(8,128)(2,1)S(1)} async-done(((bf16[32,512,64]{1,2,0:T(8,128)(2,1)}), bf16[32,512,64]{1,2,0:T(8,128)(2,1)S(1)}, u32[]{:S(2)}, u32[]{:S(2)}) %all-to-all-start.1) | async-done | bytes 2097184 | tf_op jit(solution)/shard_map/all_to_all | solution.py:21
  130.9 7.4 %all-to-all-start.2 = ((bf16[128,32,64]{0,2,1:T(8,128)(2,1)}), bf16[128,32,64]{0,2,1:T(8,128)(2,1)S(1)}, u32[]{:S(2)}, u32[]{:S(2)}) async-start(bf16[128,32,64]{0,2,1:T(8,128)(2,1)} %bitcast.51), calls=%async_computation.2 | async-start | bytes 1048576 | tf_op jit(solution)/shard_map/all_to_all | solution.py:117
  138.3 2.7 fusion.18
  142.3 13.3 %all-to-all-done.2 = bf16[128,32,64]{0,2,1:T(8,128)(2,1)S(1)} async-done(((bf16[128,32,64]{0,2,1:T(8,128)(2,1)}), bf16[128,32,64]{0,2,1:T(8,128)(2,1)S(1)}, u32[]{:S(2)}, u32[]{:S(2)}) %all-to-all-start.2) | async-done | bytes 524320 | tf_op jit(solution)/shard_map/all_to_all | solution.py:117
  156.4 4.2 all-to-all-start.3
  161.6 11.3 %all-to-all-done.3 = bf16[4,1,128,512]{3,2,1,0:T(8,128)(2,1)} async-done(((bf16[4,1,128,512]{3,2,1,0:T(8,128)(2,1)}), bf16[4,1,128,512]{3,2,1,0:T(8,128)(2,1)}, u32[]{:S(2)}, u32[]{:S(2)}) %all-to-all-start.3) | async-done | bytes 524320 | tf_op jit(solution)/shard_map/all_to_all | solution.py:16
  173.0 15.6 %all_to_all.80 = bf16[4,1,128,512]{3,2,1,0:T(8,128)(2,1)} all-to-all(bf16[4,1,128,512]{3,2,1,0:T(8,128)(2,1)S(1)} %stack.14), channel_id=1, replica_groups=mesh['rep'=2,'fs_0'=4,'fs_1'=8,'tp'=8] {'fs_0'}, dimensions={0} | all-to-all | bytes 1048576 | tf_op jit(solution)/shard_map/all_to_all | solution.py:16
  188.6 3.5 stack.13
  192.1 6.4 %all-to-all-start.4 = ((bf16[8,4,128,512]{3,2,1,0:T(8,128)(2,1)}), bf16[8,4,128,512]{3,2,1,0:T(8,128)(2,1)}, u32[]{:S(2)}, u32[]{:S(2)}) async-start(bf16[8,4,128,512]{3,2,1,0:T(8,128)(2,1)} %stack.13), calls=%async_computation.4 | async-start | bytes 8388608 | tf_op jit(solution)/shard_map/all_to_all | solution.py:16
  198.5 2.5 fusion.4
  202.8 89.2 %all-to-all-done.4 = bf16[8,4,128,512]{3,2,1,0:T(8,128)(2,1)} async-done(((bf16[8,4,128,512]{3,2,1,0:T(8,128)(2,1)}), bf16[8,4,128,512]{3,2,1,0:T(8,128)(2,1)}, u32[]{:S(2)}, u32[]{:S(2)}) %all-to-all-start.4) | async-done | bytes 4194336 | tf_op jit(solution)/shard_map/all_to_all | solution.py:16
  292.0 3.5 stack.15
  295.5 6.2 %all-to-all-start.7 = ((bf16[8,4,128,512]{3,2,1,0:T(8,128)(2,1)}), bf16[8,4,128,512]{3,2,1,0:T(8,128)(2,1)}, u32[]{:S(2)}, u32[]{:S(2)}) async-start(bf16[8,4,128,512]{3,2,1,0:T(8,128)(2,1)} %stack.15), calls=%async_computation.7 | async-start | bytes 8388608 | tf_op jit(solution)/shard_map/all_to_all | solution.py:16
  301.7 1.0 pad_maximum_fusion
  303.9 93.1 %all-to-all-done.7 = bf16[8,4,128,512]{3,2,1,0:T(8,128)(2,1)} async-done(((bf16[8,4,128,512]{3,2,1,0:T(8,128)(2,1)}), bf16[8,4,128,512]{3,2,1,0:T(8,128)(2,1)}, u32[]{:S(2)}, u32[]{:S(2)}) %all-to-all-start.7) | async-done | bytes 4194336 | tf_op jit(solution)/shard_map/all_to_all | solution.py:16
  396.9 5.8 %all-to-all-start.8 = ((bf16[128,32,64]{0,2,1:T(8,128)(2,1)}), bf16[128,32,64]{0,2,1:T(8,128)(2,1)}, u32[]{:S(2)}, u32[]{:S(2)}) async-start(bf16[128,32,64]{0,2,1:T(8,128)(2,1)} %bitcast.12), calls=%async_computation.8 | async-start | bytes 1048576 | tf_op jit(solution)/shard_map/all_to_all | solution.py:116
  402.8 2.1 slice_convert_fusion
  405.3 2.6 copy.34
  408.0 4.6 %copy.35 = bf16[8,4,128,512]{3,2,0,1:T(8,128)(2,1)} copy(bf16[8,4,128,512]{3,2,1,0:T(8,128)(2,1)} %all-to-all-done.7) | data formatting | bytes 8388608 | tf_op jit(solution)/shard_map/all_to_all | solution.py:16
  413.4 6.5 %all-to-all-done.8 = bf16[128,32,64]{0,2,1:T(8,128)(2,1)} async-done(((bf16[128,32,64]{0,2,1:T(8,128)(2,1)}), bf16[128,32,64]{0,2,1:T(8,128)(2,1)}, u32[]{:S(2)}, u32[]{:S(2)}) %all-to-all-start.8) | async-done | bytes 524320 | tf_op jit(solution)/shard_map/all_to_all | solution.py:116
  420.6 7.6 %all-to-all-start.5 = ((bf16[2,64,512]{2,1,0:T(8,128)(2,1)}), bf16[2,64,512]{2,1,0:T(8,128)(2,1)S(1)}, u32[]{:S(2)}, u32[]{:S(2)}) async-start(bf16[2,64,512]{2,1,0:T(8,128)(2,1)} %broadcast_in_dim.10), calls=%async_computation.5 | async-start | bytes 262144 | tf_op jit(solution)/shard_map/all_to_all | solution.py:21
  428.1 3.2 fusion.8
  431.4 5.2 %all-to-all-done.5 = bf16[2,64,512]{2,1,0:T(8,128)(2,1)S(1)} async-done(((bf16[2,64,512]{2,1,0:T(8,128)(2,1)}), bf16[2,64,512]{2,1,0:T(8,128)(2,1)S(1)}, u32[]{:S(2)}, u32[]{:S(2)}) %all-to-all-start.5) | async-done | bytes 131104 | tf_op jit(solution)/shard_map/all_to_all | solution.py:21
  437.2 3.4 all-to-all-start.9
  440.6 1.1 fusion.13
  443.4 5.5 %all-to-all-done.9 = bf16[2,512,64]{1,2,0:T(8,128)(2,1)S(1)} async-done(((bf16[2,512,64]{1,2,0:T(8,128)(2,1)}), bf16[2,512,64]{1,2,0:T(8,128)(2,1)S(1)}, u32[]{:S(2)}, u32[]{:S(2)}) %all-to-all-start.9) | async-done | bytes 131104 | tf_op jit(solution)/shard_map/all_to_all | solution.py:21
  (49 shorter events, 11.5 us)
Async XLA Ops:
  8.2 64.3 %copy-start.11 = (bf16[512,64]{0,1:T(8,128)(2,1)S(1)}, bf16[512,64]{0,1:T(8,128)(2,1)}, u32[]{:S(2)}) copy-start(bf16[512,64]{0,1:T(8,128)(2,1)} %param.13) | copy-start | bytes 196612
  74.1 5.1 %copy-start = (bf16[128,2048]{1,0:T(8,128)(2,1)S(1)}, bf16[128,2048]{1,0:T(8,128)(2,1)}, u32[]{:S(2)}) copy-start(bf16[128,2048]{1,0:T(8,128)(2,1)} %param.9) | copy-start | bytes 1572868
  74.1 5.3 %copy-start.2 = (bf16[128,2048]{1,0:T(8,128)(2,1)S(1)}, bf16[128,2048]{1,0:T(8,128)(2,1)}, u32[]{:S(2)}) copy-start(bf16[128,2048]{1,0:T(8,128)(2,1)} %param.8) | copy-start | bytes 1572868
  74.1 5.5 %copy-start.10 = (f32[2048]{0:T(1024)S(1)}, f32[2048]{0:T(1024)}, u32[]{:S(2)}) copy-start(f32[2048]{0:T(1024)} %param.11) | copy-start | bytes 24580
  74.1 56.8 %all-to-all-start.1 = ((bf16[32,512,64]{1,2,0:T(8,128)(2,1)}), bf16[32,512,64]{1,2,0:T(8,128)(2,1)S(1)}, u32[]{:S(2)}, u32[]{:S(2)}) async-start(bf16[32,512,64]{1,2,0:T(8,128)(2,1)} %broadcast_in_dim.9), calls=%async_computation.1 | async-start | bytes 4194304 | tf_op jit(solution)/shard_map/all_to_all | solution.py:21
  130.9 24.7 %all-to-all-start.2 = ((bf16[128,32,64]{0,2,1:T(8,128)(2,1)}), bf16[128,32,64]{0,2,1:T(8,128)(2,1)S(1)}, u32[]{:S(2)}, u32[]{:S(2)}) async-start(bf16[128,32,64]{0,2,1:T(8,128)(2,1)} %bitcast.51), calls=%async_computation.2 | async-start | bytes 1048576 | tf_op jit(solution)/shard_map/all_to_all | solution.py:117
  138.3 3.5 copy-start.3
  141.0 0.8 copy-start.6
  156.4 16.5 %all-to-all-start.3 = ((bf16[4,1,128,512]{3,2,1,0:T(8,128)(2,1)}), bf16[4,1,128,512]{3,2,1,0:T(8,128)(2,1)}, u32[]{:S(2)}, u32[]{:S(2)}) async-start(bf16[4,1,128,512]{3,2,1,0:T(8,128)(2,1)} %stack.12), calls=%async_computation.3 | async-start | bytes 1048576 | tf_op jit(solution)/shard_map/all_to_all | solution.py:16
  192.1 99.9 %all-to-all-start.4 = ((bf16[8,4,128,512]{3,2,1,0:T(8,128)(2,1)}), bf16[8,4,128,512]{3,2,1,0:T(8,128)(2,1)}, u32[]{:S(2)}, u32[]{:S(2)}) async-start(bf16[8,4,128,512]{3,2,1,0:T(8,128)(2,1)} %stack.13), calls=%async_computation.4 | async-start | bytes 8388608 | tf_op jit(solution)/shard_map/all_to_all | solution.py:16
  198.5 3.4 copy-start.7
  295.5 6.2 %copy-start.5 = (bf16[16,16,8,128]{3,1,2,0:T(8,128)(2,1)S(1)}, bf16[16,16,8,128]{3,1,2,0:T(8,128)(2,1)}, u32[]{:S(2)}) copy-start(bf16[16,16,8,128]{3,1,2,0:T(8,128)(2,1)} %copy.41) | copy-start | bytes 1572868
  295.5 101.4 %all-to-all-start.7 = ((bf16[8,4,128,512]{3,2,1,0:T(8,128)(2,1)}), bf16[8,4,128,512]{3,2,1,0:T(8,128)(2,1)}, u32[]{:S(2)}, u32[]{:S(2)}) async-start(bf16[8,4,128,512]{3,2,1,0:T(8,128)(2,1)} %stack.15), calls=%async_computation.7 | async-start | bytes 8388608 | tf_op jit(solution)/shard_map/all_to_all | solution.py:16
  301.7 1.2 copy-start.4
  301.7 101.0 %all-reduce.2.cloned.1.call-start = ((), (), s32[]{:S(2)}) async-start(), calls=%async_computation.10 | async-start | bytes 2097152 | tf_op jit(solution)/shard_map/psum | solution.py:39
  396.9 22.9 %all-to-all-start.8 = ((bf16[128,32,64]{0,2,1:T(8,128)(2,1)}), bf16[128,32,64]{0,2,1:T(8,128)(2,1)}, u32[]{:S(2)}, u32[]{:S(2)}) async-start(bf16[128,32,64]{0,2,1:T(8,128)(2,1)} %bitcast.12), calls=%async_computation.8 | async-start | bytes 1048576 | tf_op jit(solution)/shard_map/all_to_all | solution.py:116
  420.6 16.0 %all-to-all-start.5 = ((bf16[2,64,512]{2,1,0:T(8,128)(2,1)}), bf16[2,64,512]{2,1,0:T(8,128)(2,1)S(1)}, u32[]{:S(2)}, u32[]{:S(2)}) async-start(bf16[2,64,512]{2,1,0:T(8,128)(2,1)} %broadcast_in_dim.10), calls=%async_computation.5 | async-start | bytes 262144 | tf_op jit(solution)/shard_map/all_to_all | solution.py:21
  431.3 10.4 %copy-start.1 = (bf16[262144]{0:T(1024)(128)(2,1)S(1)}, bf16[262144]{0:T(1024)(128)(2,1)}, u32[]{:S(2)}) copy-start(bf16[262144]{0:T(1024)(128)(2,1)} %get-tuple-element.9) | copy-start | bytes 1572868
  431.3 11.4 %copy-start.8 = (f32[64,512]{1,0:T(8,128)S(1)}, f32[64,512]{1,0:T(8,128)}, u32[]{:S(2)}) copy-start(f32[64,512]{1,0:T(8,128)} %param.14) | copy-start | bytes 393220
  437.2 11.8 %all-to-all-start.9 = ((bf16[2,512,64]{1,2,0:T(8,128)(2,1)}), bf16[2,512,64]{1,2,0:T(8,128)(2,1)S(1)}, u32[]{:S(2)}, u32[]{:S(2)}) async-start(bf16[2,512,64]{1,2,0:T(8,128)(2,1)} %broadcast_in_dim.22), calls=%async_computation.9 | async-start | bytes 262144 | tf_op jit(solution)/shard_map/all_to_all | solution.py:21
  440.6 8.4 %copy-start.9 = (f32[512,64]{0,1:T(8,128)S(1)}, f32[512,64]{0,1:T(8,128)}, u32[]{:S(2)}) copy-start(f32[512,64]{0,1:T(8,128)} %param.15) | copy-start | bytes 393220
Sparse Core Ops, SparseCore 0:
  304.9 74.4 all-reduce.1
